TPU v7x, 32 devices: a whole 2x2x4 slice. The times are simulated.
32 devices in a mesh: sp: 8 (over z, core), tp: 4 (over y, x).
Axes of the slice: x: 2, y: 2, z: 4, core: 2. Of those that a mesh axis runs over, the one named last changes fastest.
Arguments:
- residual_in: bfloat16 [1024, 2048], P('sp', 'tp'), may hold values from -6 to 6
- query_wide: bfloat16 [1024, 2048], P('sp', 'tp'), may hold values from -6 to 6
- narrow_head_query: bfloat16 [1024, 1024], P('sp', 'tp'), may hold values from -6 to 6
- forget_wide: bfloat16 [1024, 2048], P('sp', 'tp'), may hold values from -6 to 6
- forget_narrow: bfloat16 [1024, 1024], P('sp', 'tp'), may hold values from -6 to 6
- room_wide: float32 [2048], P('tp'), as said below
- room_narrow: float32 [1024], P('tp'), as said below
- values: bfloat16 [1024, 2048], P('sp', 'tp'), may hold values from -6 to 6
- out_gate: bfloat16 [1024, 2048], P('sp', 'tp'), may hold values from -6 to 6
- head_gain: float32 [2048], P('tp'), may hold values from 0.1 to 1.9
- w_out: bfloat16 [2048, 2048], P(None, 'tp'), may hold values from -0.125 to 0.125
- norm_gain: float32 [2048], P('tp'), may hold values from 0.1 to 1.9
- route_ids: int32 [1024, 2], P('sp'), may hold values from 0 to 7, all different within a row; in each aligned block of 128 rows (0 to 127, 128 to 255, ...) at most 38 rows name the same one
- route_weight: float32 [1024, 2], P('sp'), may hold values from 0.25 to 1
- w_gate: bfloat16 [8, 2048, 4096], P('sp', None, 'tp'), may hold values from -0.125 to 0.125
- w_up: bfloat16 [8, 2048, 4096], P('sp', None, 'tp'), may hold values from -0.125 to 0.125
- w_down: bfloat16 [8, 4096, 2048], P('sp', 'tp'), may hold values from -0.09375 to 0.09375
Outputs:
- layer_out: bfloat16 [1024, 2048], P('sp', 'tp')
Inputs may be any that keep to these rules, and one draw needn't show every extreme that they name: `room_wide`: every value is positive and below 0.125. `room_narrow`: every value is positive and below 0.125. `route_ids`: each token names 2 different experts; among the 128 tokens of one index of sp no expert is named more than 38 times, and on some indices one is named exactly 38 times.
All inputs are finite; a program needn't handle non-finite values.
Results may differ from a plain program's by a relative error of at most 0.012.
Values may be sent and summed in bfloat16 or wider, within the bound.
A program may use at most 64 MiB of HBM per device.

v0:
```python
import jax
import jax.numpy as jnp
from jax import lax
from jax.sharding import PartitionSpec as P

D = 2048
DKW = 128
DKN = 64
DV = 64
TOPK = 2
BLOCK = 64


EPS = 1e-06
TOP_PRECISION = lax.Precision.HIGHEST


def run_blocks(queries, rates, contents, log_decay, block_len, initial):
    length, head_count, key_dim = queries.shape
    value_dim = contents.shape[-1]
    span_count = length // block_len

    def to_spans(tensor):
        return tensor.reshape(span_count, block_len, head_count, tensor.shape[-1]).transpose(
            0, 2, 1, 3
        )

    span_query = to_spans(queries)
    span_rate = to_spans(rates)
    span_value = to_spans(contents)
    inside = jnp.cumsum(to_spans(log_decay), axis=2)
    middle = inside[:, :, block_len // 2 - 1 : block_len // 2, :]
    ending = inside[:, :, block_len - 1 : block_len, :]
    near_query = span_query * jnp.exp(inside - middle)
    near_rate = span_rate * jnp.exp(middle - inside)
    far_query = span_query * jnp.exp(inside)
    far_rate = span_rate * jnp.exp(ending - inside)
    fading = jnp.exp(ending[:, :, 0, :])
    causal = jnp.tril(jnp.ones((block_len, block_len), jnp.float32))

    def advance(running_total, slice_pieces):
        scores = (
            jnp.einsum("htk,hsk->hts", slice_pieces[0], slice_pieces[1], precision=TOP_PRECISION)
            * causal
        )
        final_output = jnp.einsum("hts,hsv->htv", scores, slice_pieces[4], precision=TOP_PRECISION)
        final_output = final_output + jnp.einsum(
            "ncw,nws->ncs", slice_pieces[2], running_total, precision=TOP_PRECISION
        )
        running_total = slice_pieces[5][..., None] * running_total + jnp.einsum(
            "jlg,jlq->jgq", slice_pieces[3], slice_pieces[4], precision=TOP_PRECISION
        )
        return (running_total, final_output)

    final, outputs = lax.scan(
        advance, initial, (near_query, near_rate, far_query, far_rate, span_value, fading)
    )
    return (final, outputs.transpose(0, 2, 1, 3).reshape(length, head_count, value_dim))


def head_inputs(raw_query, raw_forget, room_vec, key_dim):
    length = raw_query.shape[0]
    activated = jax.nn.silu(raw_query.astype(jnp.float32)).reshape(length, -1, key_dim)
    in_rate = (room_vec * jax.nn.sigmoid(-raw_forget.astype(jnp.float32))).reshape(
        length, -1, key_dim
    )
    return (activated, in_rate, jnp.log1p(-in_rate))


def head_norm(outputs):
    return outputs * lax.rsqrt(jnp.mean(outputs * outputs, axis=-1, keepdims=True) + EPS)


def expert_apply(flat_rows, w_gate, w_up, w_down):
    gate_proj = jnp.dot(flat_rows, w_gate[0], preferred_element_type=jnp.float32)
    up_proj = jnp.dot(flat_rows, w_up[0], preferred_element_type=jnp.float32)
    hidden = (jax.nn.silu(gate_proj) * up_proj).astype(jnp.bfloat16)
    return jnp.dot(hidden, w_down[0], preferred_element_type=jnp.float32)


def body(
    residual_in,
    query_wide,
    narrow_head_query,
    forget_wide,
    forget_narrow,
    room_wide,
    room_narrow,
    values,
    out_gate,
    head_gain,
    w_out,
    norm_gain,
    route_ids,
    route_weight,
    w_gate,
    w_up,
    w_down,
):
    length = residual_in.shape[0]
    value_cols = values.astype(jnp.float32).reshape(length, -1, 2, DV)
    wide_query, wide_rate, wide_log = head_inputs(query_wide, forget_wide, room_wide, DKW)
    narrow_query, narrow_rate, narrow_log = head_inputs(
        narrow_head_query, forget_narrow, room_narrow, DKN
    )
    pair_count = wide_query.shape[1]
    wide_end, wide_out = run_blocks(
        wide_query,
        wide_rate,
        value_cols[:, :, 0],
        wide_log,
        BLOCK,
        jnp.zeros((pair_count, DKW, DV), jnp.float32),
    )
    narrow_end, narrow_out = run_blocks(
        narrow_query,
        narrow_rate,
        value_cols[:, :, 1],
        narrow_log,
        BLOCK,
        jnp.zeros((pair_count, DKN, DV), jnp.float32),
    )
    wide_sum = jnp.cumsum(wide_log, axis=0)
    narrow_sum = jnp.cumsum(narrow_log, axis=0)
    logs_all = (
        lax.all_gather(wide_sum[-1][None], "sp", axis=0, tiled=True),
        lax.all_gather(narrow_sum[-1][None], "sp", axis=0, tiled=True),
    )
    position = lax.axis_index("sp")
    wide_upto = jnp.cumsum(logs_all[0], axis=0)
    narrow_upto = jnp.cumsum(logs_all[1], axis=0)
    wide_here = wide_upto[position] - logs_all[0][position]
    narrow_here = narrow_upto[position] - logs_all[1][position]
    pieces = (
        lax.all_gather(wide_end[None], "sp", axis=0, tiled=True),
        lax.all_gather(narrow_end[None], "sp", axis=0, tiled=True),
    )
    tally_rows = pieces[0].shape[0]
    device_ids = jnp.arange(tally_rows, dtype=jnp.int32)
    before = (device_ids < position)[:, None, None]
    wide_gap = wide_here[None] - wide_upto
    narrow_gap = narrow_here[None] - narrow_upto
    wide_scale = jnp.where(before, jnp.exp(jnp.where(before, wide_gap, 0.0)), 0.0)
    narrow_scale = jnp.where(before, jnp.exp(jnp.where(before, narrow_gap, 0.0)), 0.0)
    wide_in = jnp.sum(wide_scale[..., None] * pieces[0], axis=0)
    narrow_in = jnp.sum(narrow_scale[..., None] * pieces[1], axis=0)
    wide_full = wide_out + jnp.einsum(
        "tpk,pkv->tpv", wide_query * jnp.exp(wide_sum), wide_in, precision=TOP_PRECISION
    )
    narrow_full = narrow_out + jnp.einsum(
        "tpk,pkv->tpv", narrow_query * jnp.exp(narrow_sum), narrow_in, precision=TOP_PRECISION
    )
    normed_heads = jnp.stack([head_norm(wide_full), head_norm(narrow_full)], axis=2).reshape(
        length, -1
    )
    mixed = (normed_heads * head_gain * jax.nn.silu(out_gate.astype(jnp.float32))).astype(
        jnp.bfloat16
    )
    projected = jnp.dot(
        lax.all_gather(mixed, "tp", axis=1, tiled=True), w_out, preferred_element_type=jnp.float32
    )
    residual_mid = (residual_in.astype(jnp.float32) + projected).astype(jnp.bfloat16)
    mid_float = residual_mid.astype(jnp.float32)
    squares = lax.psum(jnp.sum(mid_float * mid_float, axis=1), "tp")
    normed_cols = (mid_float * lax.rsqrt(squares / D + EPS)[:, None] * norm_gain).astype(
        jnp.bfloat16
    )
    experts = lax.axis_size("sp")
    capacity = (7 * TOPK * length + 6 * experts - 1) // (6 * experts)
    flat_ids = route_ids.reshape(-1)
    matches = (flat_ids[:, None] == jnp.arange(experts, dtype=jnp.int32)[None, :]).astype(jnp.int32)
    slot_rank = jnp.sum((jnp.cumsum(matches, axis=0) - matches) * matches, axis=1)
    positions = flat_ids * capacity + slot_rank
    owners = (
        jnp.full((experts * capacity,), length, jnp.int32)
        .at[positions]
        .set(jnp.arange(length * TOPK, dtype=jnp.int32) // TOPK)
    )
    token_rows = lax.all_gather(normed_cols, "tp", axis=1, tiled=True)
    outgoing = jnp.take(token_rows, owners, axis=0, mode="fill", fill_value=0).reshape(
        experts, capacity, -1
    )
    arrived = lax.all_to_all(outgoing, "sp", split_axis=0, concat_axis=0, tiled=True)
    flat_rows = arrived.reshape(-1, arrived.shape[-1])
    partial_value = expert_apply(flat_rows, w_gate, w_up, w_down).reshape(
        arrived.shape[0], arrived.shape[1], -1
    )
    weights_flat = route_weight.reshape(-1, 1)
    handed_back = lax.all_to_all(partial_value, "sp", split_axis=0, concat_axis=0, tiled=True)
    picked = jnp.take(handed_back.reshape(experts * capacity, -1), positions, axis=0)
    local_sum = jnp.sum((picked * weights_flat).reshape(length, TOPK, -1), axis=1)
    routed = lax.psum_scatter(local_sum, "tp", scatter_dimension=1, tiled=True)
    return (mid_float + routed).astype(jnp.bfloat16)


def solution(mesh):
    placed = (
        P("sp", "tp"),
        P("sp", "tp"),
        P("sp", "tp"),
        P("sp", "tp"),
        P("sp", "tp"),
        P("tp"),
        P("tp"),
        P("sp", "tp"),
        P("sp", "tp"),
        P("tp"),
        P(None, "tp"),
        P("tp"),
        P("sp", None),
        P("sp", None),
        P("sp", None, "tp"),
        P("sp", None, "tp"),
        P("sp", "tp", None),
    )
    return jax.shard_map(body, mesh=mesh, in_specs=placed, out_specs=P("sp", "tp"), check_vma=False)
```

profile of v0, /device:TPU:1, one launch (start us, length us, event | category | flops | bytes accessed | tf_op | source)
XLA Modules:
  0.0 304.0 jit_solution(16579221785881495350)
XLA Ops:
  13.0 1.9 bitcast_multiply_fusion.7
  15.7 6.1 %while.26 = (s32[]{:T(128)}, f32[4,128,64]{1,2,0:T(8,128)S(1)}, f32[2,4,64,64]{3,2,1,0:T(8,128)}, f32[2,4,128]{2,1,0:T(4,128)S(1)}, f32[2,4,64,128]{3,2,1,0:T(8,...) while((s32[]{:T(128)}, f32[4,128,64]{1,2,0:T(8,128)S(1)}, ...), condition=%wide.region_2.3_spmd.clone, body=%wide.region_1.2_spmd.clone.sunk | while | flops 88252416 | bytes 1696384 | solution.py:55
  28.6 14.6 %all_gather.18 = f32[8,4,128]{2,1,0:T(4,128)S(1)} all-gather(f32[1,4,128]{2,1,0:T(4,128)S(1)} %slice.47), channel_id=1, replica_groups=mesh['sp'=8,'tp'=4] {'sp'}, dimensions={0}, use_global_device_ids=true | all-gather | bytes 18432 | tf_op jit(solution)/shard_map/all_gather | solution.py:126
  49.1 1.9 bitcast_multiply_fusion.3
  51.7 7.5 %while.27 = (s32[]{:T(128)}, f32[4,64,64]{2,1,0:T(8,128)S(1)}, f32[2,4,64,64]{3,2,1,0:T(8,128)}, f32[2,4,64]{2,1,0:T(4,128)}, f32[2,4,64,64]{3,2,1,0:T(8,128)}, ...) while((s32[]{:T(128)}, f32[4,64,64]{2,1,0:T(8,128)S(1)}, ...), condition=%wide.region_9.10_spmd.clone, body=%wide.region_8.9_spmd.clone.sunk | while | flops 50438144 | bytes 1562240 | solution.py:55
  60.5 12.8 %all_gather.20 = f32[8,4,64]{2,1,0:T(4,128)S(1)} all-gather(f32[1,4,64]{2,1,0:T(4,128)S(1)} %slice.51), channel_id=1, replica_groups=mesh['sp'=8,'tp'=4] {'sp'}, dimensions={0}, use_global_device_ids=true | all-gather | bytes 9216 | tf_op jit(solution)/shard_map/all_gather | solution.py:127
  79.6 1.7 copy.122
  83.4 17.1 %all-gather.1 = f32[32,64,64]{2,1,0:T(8,128)S(1)} all-gather(f32[4,64,64]{2,1,0:T(8,128)S(1)} %get-tuple-element.114), channel_id=3, replica_groups=mesh['sp'=8,'tp'=4] {'sp'}, dimensions={0}, use_global_device_ids=true | all-gather | bytes 589824 | tf_op jit(solution)/shard_map/all_gather | solution.py:136
  105.2 9.1 %all_gather.22 = bf16[128,2048]{0,1:T(8,128)(2,1)S(1)} all-gather(bf16[128,512]{0,1:T(8,128)(2,1)S(1)} %fusion.65), channel_id=1, replica_groups=mesh['sp'=8,'tp'=4] {'tp'}, dimensions={1}, use_global_device_ids=true | all-gather | bytes 655360 | tf_op jit(solution)/shard_map/all_gather | solution.py:160
  114.9 7.1 %psum.7 = f32[128]{0:T(128)S(1)} all-reduce(f32[128]{0:T(128)S(1)} %get-tuple-element.304), channel_id=1, replica_groups=mesh['sp'=8,'tp'=4] {'tp'}, use_global_device_ids=true, to_apply=%region_19.20 | all-reduce | flops 128 | bytes 1024 | tf_op jit(solution)/shard_map/psum | solution.py:164
  122.1 8.6 %all_gather.23 = bf16[128,2048]{1,0:T(8,128)(2,1)S(1)} all-gather(bf16[128,512]{1,0:T(8,128)(2,1)S(1)} %multiply_convert_fusion), channel_id=1, replica_groups=mesh['sp'=8,'tp'=4] {'tp'}, dimensions={1}, use_global_device_ids=true | all-gather | bytes 655360 | tf_op jit(solution)/shard_map/all_gather | solution.py:179
  130.7 3.0 gather_fusion
  135.3 38.5 %all_to_all.10 = bf16[8,38,2048]{2,1,0:T(8,128)(2,1)S(1)} all-to-all(bf16[8,38,2048]{2,1,0:T(8,128)(2,1)S(1)} %broadcast_select_fusion), channel_id=1, replica_groups=mesh['sp'=8,'tp'=4] {'sp'}, dimensions={0} | all-to-all | bytes 2490368 | tf_op jit(solution)/shard_map/all_to_all | solution.py:183
  175.0 4.2 %fusion.44 = f32[304,1024]{1,0:T(8,128)S(1)} fusion(bf16[304,2048]{1,0:T(8,128)(2,1)} %reshape.178, bf16[1,2048,1024]{2,1,0:T(8,128)(2,1)} %param.35), kind=kOutput, calls=%fused_computation.57 | convolution fusion | flops 1275068416 | bytes 6684672 | tf_op jit(solution)/shard_map/dot_general | solution.py:75
  179.2 1.6 fusion.49
  181.0 5.2 %fusion.40 = f32[8,38,2048]{2,1,0:T(8,128)} fusion(bf16[8,38,1024]{2,1,0:T(8,128)(2,1)S(1)} %dot_general.49, bf16[1,1024,2048]{2,1,0:T(8,128)(2,1)} %param.37), kind=kOutput, calls=%fused_computation.53 | convolution fusion | flops 1275068416 | bytes 7307264 | tf_op jit(solution)/shard_map/dot_general | solution.py:78
  186.2 5.5 %all-to-all-start.1 = ((f32[8,38,2048]{2,1,0:T(8,128)}), f32[8,38,2048]{2,1,0:T(8,128)}, u32[]{:S(2)}, u32[]{:S(2)}) async-start(f32[8,38,2048]{2,1,0:T(8,128)} %fusion.40), calls=%async_computation.1 | async-start | bytes 5242880 | tf_op jit(solution)/shard_map/all_to_all | solution.py:189
  192.2 58.9 %all-to-all-done.1 = f32[8,38,2048]{2,1,0:T(8,128)} async-done(((f32[8,38,2048]{2,1,0:T(8,128)}), f32[8,38,2048]{2,1,0:T(8,128)}, u32[]{:S(2)}, u32[]{:S(2)}) %all-to-all-start.1) | async-done | bytes 2490400 | tf_op jit(solution)/shard_map/all_to_all | solution.py:189
  251.1 2.9 reshape.179
  254.1 5.3 %gather_fusion.1 = f32[256,2048]{1,0:T(8,128)} fusion(f32[304,2048]{1,0:T(8,128)} %reshape.179, s32[1024]{0:T(1024)S(1)} %pad_clamp_fusion), kind=kCustom, calls=%fused_computation.1 | custom fusion | bytes 4195328 | tf_op jit(solution)/shard_map/jit(_take)/gather | solution.py:190
  259.4 3.5 %gather.15 = f32[128,2,2048]{2,1,0:T(2,128)} reshape(f32[256,2048]{1,0:T(8,128)} %gather_fusion.1) | data formatting | bytes 4194304 | tf_op jit(solution)/shard_map/jit(_take)/gather | solution.py:190
  262.8 6.5 %multiply_reduce_fusion = f32[128,2048]{1,0:T(8,128)} fusion(f32[128,2,2048]{2,1,0:T(2,128)} %gather.15, pred[128,2]{1,0:T(8,128)(4,1)S(1)} %copy.126, f32[128,2]{1,0:T(8,128)S(1)} %copy.128), kind=kLoop, calls=%fused_computation.59 | loop fusion | flops 1310720 | bytes 3147008 | tf_op jit(solution)/shard_map/reduce_sum | solution.py:191
  269.4 26.1 %reduce-scatter.2.cloned.1.call-done = f32[128,512]{1,0:T(8,128)} async-done(((f32[128,2048]{1,0:T(8,128)}), f32[128,512]{1,0:T(8,128)}) %reduce-scatter.2.cloned.1.call-update) | async-done | bytes 262160 | tf_op jit(solution)/shard_map/reduce_scatter | solution.py:192
  295.5 1.6 add_convert_fusion
  (210 shorter events, 52.1 us)
Async XLA Ops:
  6.5 107.8 %copy-start = (bf16[2048,512]{1,0:T(8,128)(2,1)S(1)}, bf16[2048,512]{1,0:T(8,128)(2,1)}, u32[]{:S(2)}) copy-start(bf16[2048,512]{1,0:T(8,128)(2,1)} %param.31) | copy-start | bytes 6291460
  6.5 96.4 %all-gather.4.cloned.1.call-start = ((), (), s32[]{:S(2)}) async-start(), calls=%async_computation.4 | async-start | bytes 1179648 | tf_op jit(solution)/shard_map/all_gather | solution.py:135
  15.7 6.8 %copy-start.26 = (s32[128,2]{0,1:T(2,128)S(1)}, s32[128,2]{0,1:T(2,128)}, u32[]{:S(2)}) copy-start(s32[128,2]{0,1:T(2,128)} %param.33) | copy-start | bytes 3076
  22.6 24.4 %copy-start.23 = (bf16[128,256]{1,0:T(8,128)(2,1)S(1)}, bf16[128,256]{1,0:T(8,128)(2,1)}, u32[]{:S(2)}) copy-start(bf16[128,256]{1,0:T(8,128)(2,1)} %param.23) | copy-start | bytes 196612
  28.6 20.2 %copy-start.16 = (f32[128,4,1,64]{0,3,2,1:T(8,128)S(1)}, f32[128,4,1,64]{0,3,2,1:T(8,128)}, u32[]{:S(2)}) copy-start(f32[128,4,1,64]{0,3,2,1:T(8,128)} %get-tuple-element.297) | copy-start | bytes 393220
  43.2 5.9 %copy-start.21 = (f32[8,4,128]{2,1,0:T(4,128)}, f32[8,4,128]{2,1,0:T(4,128)S(1)}, u32[]{:S(2)}) copy-start(f32[8,4,128]{2,1,0:T(4,128)S(1)} %all_gather.18) | copy-start | bytes 49156
  59.2 19.0 %copy-start.3 = (f32[128,512]{0,1:T(8,128)S(1)}, f32[128,512]{0,1:T(8,128)}, u32[]{:S(2)}) copy-start(f32[128,512]{0,1:T(8,128)} %copy-done.2) | copy-start | bytes 786436
  59.2 19.1 %copy-start.14 = (f32[2,4,64,64]{3,2,1,0:T(8,128)S(1)}, f32[2,4,64,64]{3,2,1,0:T(8,128)}, u32[]{:S(2)}) copy-start(f32[2,4,64,64]{3,2,1,0:T(8,128)} %get-tuple-element.113) | copy-start | bytes 393220
  59.2 20.1 %copy-start.9 = (f32[128,256]{0,1:T(8,128)S(1)}, f32[128,256]{0,1:T(8,128)}, u32[]{:S(2)}) copy-start(f32[128,256]{0,1:T(8,128)} %copy-done.8) | copy-start | bytes 393220
  79.5 21.3 %copy-start.15 = (f32[128,4,64]{0,2,1:T(8,128)S(1)}, f32[128,4,64]{0,2,1:T(8,128)}, u32[]{:S(2)}) copy-start(f32[128,4,64]{0,2,1:T(8,128)} %reshape.173) | copy-start | bytes 393220
  79.5 23.3 %copy-start.13 = (f32[128,4,128]{2,1,0:T(4,128)S(1)}, f32[128,4,128]{2,1,0:T(4,128)}, u32[]{:S(2)}) copy-start(f32[128,4,128]{2,1,0:T(4,128)} %copy-done.12) | copy-start | bytes 786436
  82.5 19.6 %copy-start.31 = (f32[4,128]{1,0:T(4,128)S(1)}, f32[4,128]{1,0:T(4,128)}, u32[]{:S(2)}) copy-start(f32[4,128]{1,0:T(4,128)} %subtract_bitcast_fusion.1) | copy-start | bytes 6148
  82.6 19.6 %copy-start.36 = (pred[8]{0:T(512)(128)(4,1)S(1)}, pred[8]{0:T(512)(128)(4,1)}, u32[]{:S(2)}) copy-start(pred[8]{0:T(512)(128)(4,1)} %iota_compare_fusion.4) | copy-start | bytes 28
  102.9 11.4 %copy-start.18 = (bf16[128,512]{1,0:T(8,128)(2,1)S(1)}, bf16[128,512]{1,0:T(8,128)(2,1)}, u32[]{:S(2)}) copy-start(bf16[128,512]{1,0:T(8,128)(2,1)} %param.21) | copy-start | bytes 393220
  105.1 16.9 %copy-start.35 = (f32[512]{0:T(512)S(1)}, f32[512]{0:T(512)}, u32[]{:S(2)}) copy-start(f32[512]{0:T(512)} %param.32) | copy-start | bytes 6148
  114.3 16.3 %copy-start.25 = (s32[1024]{0:T(1024)S(1)}, s32[1024]{0:T(1024)}, u32[]{:S(2)}) copy-start(s32[1024]{0:T(1024)} %pad_clamp_fusion.1) | copy-start | bytes 12292
  114.9 7.1 %copy-start.4 = (f32[128,512]{1,0:T(8,128)}, f32[128,512]{1,0:T(8,128)S(1)}, u32[]{:S(2)}) copy-start(f32[128,512]{1,0:T(8,128)S(1)} %get-tuple-element.305) | copy-start | bytes 786436
  186.2 5.5 %copy-start.29 = (s32[256]{0:T(256)S(1)}, s32[256]{0:T(256)}, u32[]{:S(2)}) copy-start(s32[256]{0:T(256)} %copy-done.28) | copy-start | bytes 3076
  186.2 5.7 %copy-start.27 = (s32[128,2]{0,1:T(2,128)S(1)}, s32[128,2]{0,1:T(2,128)}, u32[]{:S(2)}) copy-start(s32[128,2]{0,1:T(2,128)} %param.33) | copy-start | bytes 3076
  186.2 5.9 %copy-start.37 = (f32[128,2]{0,1:T(2,128)S(1)}, f32[128,2]{0,1:T(2,128)}, u32[]{:S(2)}) copy-start(f32[128,2]{0,1:T(2,128)} %param.34) | copy-start | bytes 3076
  186.2 6.0 %copy-start.33 = (s32[256,1]{0,1:T(1,128)S(1)}, s32[256,1]{0,1:T(1,128)}, u32[]{:S(2)}) copy-start(s32[256,1]{0,1:T(1,128)} %copy-done.32) | copy-start | bytes 3076
  186.2 64.9 %all-to-all-start.1 = ((f32[8,38,2048]{2,1,0:T(8,128)}), f32[8,38,2048]{2,1,0:T(8,128)}, u32[]{:S(2)}, u32[]{:S(2)}) async-start(f32[8,38,2048]{2,1,0:T(8,128)} %fusion.40), calls=%async_computation.1 | async-start | bytes 5242880 | tf_op jit(solution)/shard_map/all_to_all | solution.py:189
  191.7 103.9 %reduce-scatter.2.cloned.1.call-start = ((), (), s32[]{:S(2)}) async-start(), calls=%async_computation.3 | async-start | bytes 1310720 | tf_op jit(solution)/shard_map/reduce_scatter | solution.py:192
  262.8 32.7 %copy-start.5 = (f32[128,512]{1,0:T(8,128)S(1)}, f32[128,512]{1,0:T(8,128)}, u32[]{:S(2)}) copy-start(f32[128,512]{1,0:T(8,128)} %copy-done.4) | copy-start | bytes 786436
  (19 other events, 42.9 us)
Sparse Core Ops, SparseCore 0:
  22.6 24.6 all-gather.3
  269.5 25.9 reduce-scatter.1
where the time goes:
time: 306 us; the launch traced here: 304 us
  blocking collectives  108 us (35%)
  waiting for transfers between devices  85.1 us (28%)
  local copies, waits for them, and re-layouts  41 us (13%)
  other arithmetic  26.1 us (9%)
  matrix products  24.3 us (8%)
  between operations  14.1 us (5%)
  starting transfers between devices  5.46 us (2%)
    all_to_all x1, waiting for transfers between devices, body(): lax.all_to_all(partial_value, 'sp', split_axis=0, concat_axis=0, tiled=True)  58.9 us
    all_to_all x1, blocking collectives, body(): lax.all_to_all(outgoing, 'sp', split_axis=0, concat_axis=0, tiled=True)  38.5 us
    reduce_scatter x1, waiting for transfers between devices, body(): routed = lax.psum_scatter(local_sum, 'tp', scatter_dimension=1, tiled=True)  26.1 us
    all_gather x1, blocking collectives, body(): lax.all_gather(narrow_end[None], 'sp', axis=0, tiled=True)  17.1 us
    all_gather x1, blocking collectives, body(): lax.all_gather(wide_sum[-1][None], 'sp', axis=0, tiled=True)  14.6 us
    all_gather x1, blocking collectives, body(): lax.all_gather(narrow_sum[-1][None], 'sp', axis=0, tiled=True)  12.8 us
    all_gather x1, blocking collectives, body(): lax.all_gather(mixed, 'tp', axis=1, tiled=True)  9.09 us
    gather x2, local copies, waits for them, and re-layouts, body(): jnp.take(handed_back.reshape(experts * capacity, -1), positions, axis=0)  8.77 us
  transfers between devices with their start and end apart: 3, of which 2 were waited for; matrix products, arithmetic and copies ran while one was open for 12% of the time, Pallas kernels for 0%

commit v1 on v0

v1 whole, which is shorter than its diff:
```python
import jax
import jax.numpy as jnp
from jax import lax
from jax.experimental import pallas as pl
from jax.experimental.pallas import tpu as pltpu
from jax.sharding import PartitionSpec as P

DKW = 128
DKN = 64
DV = 64
TOPK = 2
LANES = 128
ROWS = 16
EPS = 1e-06
F32 = jnp.float32
BF16 = jnp.bfloat16


def silu(v):
    return v / (1.0 + jnp.exp(-v))


def dot(a, b):
    return lax.dot_general(a, b, (((1,), (0,)), ((), ())), preferred_element_type=F32)


def dot_nt(a, b):
    return lax.dot_general(a, b, (((1,), (1,)), ((), ())), preferred_element_type=F32)


def remote(src, dst, send, recv, **where):
    return pltpu.make_async_remote_copy(
        src_ref=src,
        dst_ref=dst,
        send_sem=send,
        recv_sem=recv,
        device_id=where,
        device_id_type=pl.DeviceIdType.MESH,
    )


def greet(n_sp, n_tp, sp, tp):
    barrier = pltpu.get_barrier_semaphore()
    for d in range(1, n_sp):
        pl.semaphore_signal(
            barrier,
            inc=1,
            device_id={"sp": lax.rem(sp + d, n_sp)},
            device_id_type=pl.DeviceIdType.MESH,
        )
    for d in range(1, n_tp):
        pl.semaphore_signal(
            barrier,
            inc=1,
            device_id={"tp": lax.rem(tp + d, n_tp)},
            device_id_type=pl.DeviceIdType.MESH,
        )
    return barrier


def front_kernel(
    n_sp,
    n_tp,
    qw,
    qn,
    fw,
    fn,
    rw,
    rn,
    values,
    gate,
    gain,
    w_out,
    residual,
    norm_gain,
    pick,
    mid_out,
    rows_out,
    pack,
    partner,
    chip,
    chips,
    half_in,
    half_got,
    state_in,
    far_q,
    local_out,
    mixed,
    mixbuf,
    squares,
    sqbuf,
    outgoing,
    psem,
    csem,
    crem,
    hsem,
    msem,
    mrem,
    qsem,
    qrem,
    asem,
    arem,
    fsem,
    frem,
):
    sp = lax.axis_index("sp")
    tp = lax.axis_index("tp")
    barrier = greet(n_sp, n_tp, sp, tp)
    length = qw.shape[0]
    wide = qw.shape[1]
    lanes = wide + qn.shape[1]
    pairs = wide // DKW
    cols = residual.shape[1]
    cap = rows_out.shape[0] // n_sp
    n_z = n_sp // 2
    core = lax.rem(sp, 2)
    z = sp // 2

    row = lax.broadcasted_iota(jnp.int32, (length, length), 0)
    col = lax.broadcasted_iota(jnp.int32, (length, length), 1)
    causal = row >= col
    tri = jnp.where(causal, 1.0, 0.0).astype(BF16)
    low = lax.broadcasted_iota(jnp.int32, (1, LANES), 1) < DV

    def prepare(q_ref, f_ref, room_ref, at):
        q = silu(q_ref[:, at].astype(F32))
        rate = room_ref[:, at] / (1.0 + jnp.exp(f_ref[:, at].astype(F32)))
        log = jnp.log1p(-rate)
        high = log.astype(BF16)
        inside = dot(tri, high) + dot(tri, (log - high.astype(F32)).astype(BF16))
        middle = inside[length // 2 - 1 : length // 2]
        ending = inside[length - 1 : length]
        up = jnp.exp(inside - middle)
        near_q = q * up
        near_r = (rate * jnp.exp(middle - inside)).astype(BF16)
        return (
            near_q,
            near_r,
            (q * jnp.exp(inside)).astype(BF16),
            (rate * jnp.exp(ending - inside)).astype(BF16),
            jnp.exp(ending),
        )

    group_sets = []
    for g in range((lanes - wide) // LANES):
        at = slice(g * LANES, (g + 1) * LANES)
        group_sets.append(prepare(qn, fn, rn, at))
    narrow_states = [None] * len(group_sets)
    for p in range(pairs):
        at = slice(p * LANES, (p + 1) * LANES)
        v = values[:, at]
        v_t = v.astype(F32).T.astype(BF16)
        near_q, near_r, fq, fr, fade = prepare(qw, fw, rw, at)
        scores = jnp.where(causal, dot_nt(near_q.astype(BF16), near_r), 0.0).astype(BF16)
        wide_out = dot(scores, v)
        far_q[:, at] = fq
        pack[:DV, at] = dot(v_t, fr)[:DV].astype(BF16)
        pack[DV:, at] = jnp.broadcast_to(fade, (ROWS, LANES)).astype(BF16)
        near_q, near_r, fq, fr, fade = group_sets[p // 2]
        mine = low if p % 2 == 0 else ~low
        scores = dot_nt(jnp.where(mine, near_q, 0.0).astype(BF16), near_r)
        narrow_out = dot(jnp.where(causal, scores, 0.0).astype(BF16), v)
        local_out[:, at] = jnp.where(low, wide_out, narrow_out)
        piece = jnp.where(mine, dot(v_t, fr)[DV:], 0.0)
        held = narrow_states[p // 2]
        narrow_states[p // 2] = piece if held is None else held + piece
    for g, (_, _, fq, _, fade) in enumerate(group_sets):
        at = slice(wide + g * LANES, wide + (g + 1) * LANES)
        far_q[:, at] = fq
        pack[:DV, at] = narrow_states[g].astype(BF16)
        pack[DV:, at] = jnp.broadcast_to(fade, (ROWS, LANES)).astype(BF16)

    pl.semaphore_wait(barrier, n_sp - 1 + n_tp - 1)
    other = sp + 1 - 2 * core
    to_partner = remote(pack, partner, psem.at[0], psem.at[1], sp=other)
    to_partner.start()
    to_partner.wait()
    half = lanes // 2
    mine = pl.ds(pl.multiple_of(core * half, LANES), half)
    theirs = pl.ds(pl.multiple_of((1 - core) * half, LANES), half)
    own = pack[:, mine].astype(F32)
    far = partner[:, mine].astype(F32)
    first = jnp.where(core == 0, own, far)
    second = jnp.where(core == 0, far, own)
    chip[:DV, :] = (second[DV : DV + 1] * first[:DV] + second[:DV]).astype(BF16)
    chip[DV:, :] = (second[DV:] * first[DV:]).astype(BF16)

    def chip_copy(d):
        return remote(
            chip, chips.at[z], csem.at[d], crem.at[d], sp=lax.rem(z + d, n_z) * 2 + core
        )

    for d in range(1, n_z):
        chip_copy(d).start()
    chips[z] = chip[...]
    for d in range(1, n_z):
        chip_copy(d).wait()
    total = jnp.zeros((DV, half), F32)
    for s in range(n_z):
        piece = chips[s].astype(F32)
        total = jnp.where(s < z, piece[DV : DV + 1] * total + piece[:DV], total)
    half_in[...] = total
    to_partner = remote(half_in, half_got, hsem.at[0], hsem.at[1], sp=other)
    to_partner.start()
    to_partner.wait()

    def enter(part, at):
        prior = partner[:, at].astype(F32)
        moved = prior[DV : DV + 1] * part + prior[:DV]
        state_in[:, at] = jnp.where(core == 1, moved, part).astype(BF16)

    enter(total, mine)
    enter(half_got[...], theirs)

    blank = jnp.zeros((DV, LANES), BF16)
    for p in range(pairs):
        at = slice(p * LANES, (p + 1) * LANES)
        g_at = slice(wide + p // 2 * LANES, wide + (p // 2 + 1) * LANES)
        keep = low if p % 2 == 0 else ~low
        narrow = jnp.where(keep, state_in[:, g_at], jnp.zeros((), BF16))
        out = local_out[:, at]
        out = out + dot_nt(far_q[:, at], jnp.concatenate([state_in[:, at], blank], axis=0))
        out = out + dot_nt(far_q[:, g_at], jnp.concatenate([blank, narrow], axis=0))
        sq = out * out
        wide_mean = jnp.sum(jnp.where(low, sq, 0.0), axis=1, keepdims=True) / DV
        narrow_mean = jnp.sum(jnp.where(low, 0.0, sq), axis=1, keepdims=True) / DV
        scale = lax.rsqrt(jnp.where(low, wide_mean, narrow_mean) + EPS)
        mixed[:, at] = (out * scale * gain[:, at] * silu(gate[:, at].astype(F32))).astype(BF16)

    width = mixed.shape[1]

    def mix_copy(d):
        return remote(mixed, mixbuf.at[d], msem.at[d], mrem.at[d], tp=lax.rem(tp + d, n_tp))

    for d in range(1, n_tp):
        mix_copy(d).start()

    def weight_rows(owner):
        return w_out[pl.ds(pl.multiple_of(owner * width, LANES), width), :]

    acc = residual[...].astype(F32)
    proj = dot(mixed[...], weight_rows(tp))
    for d in range(1, n_tp):
        mix_copy(d).wait()
        proj = proj + dot(mixbuf[d], weight_rows(lax.rem(tp + n_tp - d, n_tp)))
    mid = (acc + proj).astype(BF16)
    mid_out[...] = mid
    mid = mid.astype(F32)
    squares[...] = jnp.broadcast_to(jnp.sum(mid * mid, axis=1, keepdims=True), squares.shape)

    def sq_copy(d):
        return remote(squares, sqbuf.at[d], qsem.at[d], qrem.at[d], tp=lax.rem(tp + d, n_tp))

    for d in range(1, n_tp):
        sq_copy(d).start()
    total_sq = squares[...]
    for d in range(1, n_tp):
        sq_copy(d).wait()
        total_sq = total_sq + sqbuf[d]
    scale = lax.rsqrt(total_sq[:, :1] / (cols * n_tp) + EPS)
    normed = (mid * scale * norm_gain[...]).astype(BF16)
    outgoing[...] = dot(pick[...], normed).astype(BF16)

    def block(ref, owner, width_at):
        return ref.at[pl.ds(pl.multiple_of(owner * cap, ROWS), cap), width_at]

    here = pl.ds(pl.multiple_of(tp * cols, LANES), cols)
    whole = slice(None)

    def send_copy(d):
        peer = lax.rem(sp + d, n_sp)
        return remote(
            block(outgoing, peer, whole), block(rows_out, sp, here), asem.at[d], arem.at[d], sp=peer
        )

    def forward_copy(d, k):
        place = block(rows_out, lax.rem(sp + n_sp - d, n_sp), here)
        return remote(place, place, fsem.at[d, k], frem.at[d, k], tp=lax.rem(tp + k, n_tp))

    def own_copy(k):
        return remote(
            block(outgoing, sp, whole),
            block(rows_out, sp, here),
            fsem.at[0, k],
            frem.at[0, k],
            tp=lax.rem(tp + k, n_tp),
        )

    def start_send(d, carry):
        send_copy(d).start()
        return carry

    lax.fori_loop(1, n_sp, start_send, 0)
    for k in range(1, n_tp):
        own_copy(k).start()
    mine_rows = pl.ds(pl.multiple_of(sp * cap, ROWS), cap)
    rows_out[mine_rows, here] = outgoing[mine_rows, :]

    def pass_on(d, carry):
        send_copy(d).wait_recv()
        for k in range(1, n_tp):
            forward_copy(d, k).start()
        return carry

    lax.fori_loop(1, n_sp, pass_on, 0)

    def finish(d, carry):
        send_copy(d).wait_send()
        for k in range(1, n_tp):
            forward_copy(d, k).wait()
        return carry

    for k in range(1, n_tp):
        own_copy(k).wait()
    lax.fori_loop(1, n_sp, finish, 0)


def back_kernel(
    n_sp, n_tp, part, high, low, mid, out, pieces, summed, returned, rsem, rrem, bsem, brem
):
    sp = lax.axis_index("sp")
    tp = lax.axis_index("tp")
    barrier = greet(n_sp, n_tp, sp, tp)
    cols = mid.shape[1]
    cap = part.shape[0] // n_sp
    pl.semaphore_wait(barrier, n_sp - 1 + n_tp - 1)

    def rows_of(d):
        return pl.ds(pl.multiple_of(lax.rem(sp + d, n_sp) * cap, ROWS), cap)

    def cols_of(owner):
        return pl.ds(pl.multiple_of(owner * cols, LANES), cols)

    def reduce_copy(d, k):
        peer = lax.rem(tp + k, n_tp)
        return remote(
            part.at[rows_of(d), cols_of(peer)],
            pieces.at[k - 1, rows_of(d), :],
            rsem.at[d, k],
            rrem.at[d, k],
            tp=peer,
        )

    def start_reduce(d, carry):
        for k in range(1, n_tp):
            reduce_copy(lax.rem(d, n_sp), k).start()
        return carry

    lax.fori_loop(1, n_sp + 1, start_reduce, 0)

    def back_copy(d):
        peer = lax.rem(sp + d, n_sp)
        return remote(
            summed.at[rows_of(d), :],
            returned.at[rows_of(0), :],
            bsem.at[d],
            brem.at[d],
            sp=peer,
        )

    def add_up(d):
        total = part[rows_of(d), cols_of(tp)].astype(F32)
        for k in range(1, n_tp):
            reduce_copy(d, k).wait_recv()
            total = total + pieces[k - 1, rows_of(d), :].astype(F32)
        return total.astype(BF16)

    def pass_back(d, carry):
        summed[rows_of(d), :] = add_up(d)
        back_copy(d).start()
        return carry

    lax.fori_loop(1, n_sp, pass_back, 0)
    returned[rows_of(0), :] = add_up(0)

    def finish(d, carry):
        back_copy(d).wait()
        return carry

    lax.fori_loop(1, n_sp, finish, 0)

    def drain(d, carry):
        for k in range(1, n_tp):
            reduce_copy(d, k).wait_send()
        return carry

    lax.fori_loop(0, n_sp, drain, 0)
    rows = returned[...]
    moe = dot(high[...], rows) + dot(low[...], rows)
    out[...] = (mid[...].astype(F32) + moe).astype(BF16)


def vmem(count):
    return [pl.BlockSpec(memory_space=pltpu.VMEM)] * count


def body(
    residual_in,
    query_wide,
    narrow_head_query,
    forget_wide,
    forget_narrow,
    room_wide,
    room_narrow,
    values,
    out_gate,
    head_gain,
    w_out,
    norm_gain,
    route_ids,
    route_weight,
    w_gate,
    w_up,
    w_down,
):
    n_sp = lax.axis_size("sp")
    n_tp = lax.axis_size("tp")
    length, cols = residual_in.shape
    model = cols * n_tp
    width = values.shape[1]
    capacity = (7 * TOPK * length + 6 * n_sp - 1) // (6 * n_sp)
    cap = -(-capacity // ROWS) * ROWS
    slots = n_sp * cap
    room_narrow = room_narrow[None]
    narrow = room_narrow.shape[1]
    fill = -narrow % LANES
    if fill:
        edge = ((0, 0), (0, fill))
        narrow_head_query = jnp.pad(narrow_head_query, edge)
        forget_narrow = jnp.pad(forget_narrow, edge)
        room_narrow = jnp.pad(room_narrow, edge)
    lanes = query_wide.shape[1] + narrow + fill

    slot = jnp.arange(slots, dtype=jnp.int32)
    hits = route_ids[:, :, None] == (slot // cap)[None, None, :]
    named = jnp.any(hits, axis=1)
    weight = jnp.sum(jnp.where(hits, route_weight[:, :, None], 0.0), axis=1)
    earlier = jnp.tril(jnp.ones((length, length), BF16), -1)
    rank = jnp.dot(earlier, named.astype(BF16), preferred_element_type=F32)
    placed = named & (rank.astype(jnp.int32) == (slot % cap)[None, :])
    pick = placed.astype(BF16).T
    weight = jnp.where(placed, weight, 0.0)
    high = weight.astype(BF16)
    low = (weight - high.astype(F32)).astype(BF16)

    dma = pltpu.SemaphoreType.DMA
    depth = DV + ROWS
    n_z = n_sp // 2
    mid, rows = pl.pallas_call(
        lambda *refs: front_kernel(n_sp, n_tp, *refs),
        out_shape=(
            jax.ShapeDtypeStruct((length, cols), BF16),
            jax.ShapeDtypeStruct((slots, model), BF16),
        ),
        in_specs=vmem(13),
        out_specs=tuple(vmem(2)),
        scratch_shapes=[
            pltpu.VMEM((depth, lanes), BF16),
            pltpu.VMEM((depth, lanes), BF16),
            pltpu.VMEM((depth, lanes // 2), BF16),
            pltpu.VMEM((n_z, depth, lanes // 2), BF16),
            pltpu.VMEM((DV, lanes // 2), F32),
            pltpu.VMEM((DV, lanes // 2), F32),
            pltpu.VMEM((DV, lanes), BF16),
            pltpu.VMEM((length, lanes), BF16),
            pltpu.VMEM((length, width), F32),
            pltpu.VMEM((length, width), BF16),
            pltpu.VMEM((n_tp, length, width), BF16),
            pltpu.VMEM((length, LANES), F32),
            pltpu.VMEM((n_tp, length, LANES), F32),
            pltpu.VMEM((slots, cols), BF16),
            dma((2,)),
            dma((n_z,)),
            dma((n_z,)),
            dma((2,)),
            dma((n_tp,)),
            dma((n_tp,)),
            dma((n_tp,)),
            dma((n_tp,)),
            dma((n_sp,)),
            dma((n_sp,)),
            dma((n_sp, n_tp)),
            dma((n_sp, n_tp)),
        ],
        compiler_params=pltpu.CompilerParams(collective_id=0, has_side_effects=True),
        name="front",
    )(
        query_wide,
        narrow_head_query,
        forget_wide,
        forget_narrow,
        room_wide[None],
        room_narrow,
        values,
        out_gate,
        head_gain[None],
        w_out,
        residual_in,
        norm_gain[None],
        pick,
    )
    gate_proj = jnp.dot(rows, w_gate[0], preferred_element_type=F32)
    up_proj = jnp.dot(rows, w_up[0], preferred_element_type=F32)
    hidden = (jax.nn.silu(gate_proj) * up_proj).astype(BF16)
    part = jnp.dot(hidden, w_down[0], preferred_element_type=F32).astype(BF16)
    return pl.pallas_call(
        lambda *refs: back_kernel(n_sp, n_tp, *refs),
        out_shape=jax.ShapeDtypeStruct((length, cols), BF16),
        in_specs=vmem(4),
        out_specs=vmem(1)[0],
        scratch_shapes=[
            pltpu.VMEM((n_tp - 1, slots, cols), BF16),
            pltpu.VMEM((slots, cols), BF16),
            pltpu.VMEM((slots, cols), BF16),
            dma((n_sp, n_tp)),
            dma((n_sp, n_tp)),
            dma((n_sp,)),
            dma((n_sp,)),
        ],
        compiler_params=pltpu.CompilerParams(collective_id=1, has_side_effects=True),
        name="back",
    )(part, high, low, mid)


def solution(mesh):
    placed = (
        P("sp", "tp"),
        P("sp", "tp"),
        P("sp", "tp"),
        P("sp", "tp"),
        P("sp", "tp"),
        P("tp"),
        P("tp"),
        P("sp", "tp"),
        P("sp", "tp"),
        P("tp"),
        P(None, "tp"),
        P("tp"),
        P("sp", None),
        P("sp", None),
        P("sp", None, "tp"),
        P("sp", None, "tp"),
        P("sp", "tp", None),
    )
    return jax.shard_map(body, mesh=mesh, in_specs=placed, out_specs=P("sp", "tp"), check_vma=False)
```

time: 306 us -> 96.9 us (0.32)
  blocking collectives: 108 us -> 0 us
  waiting for transfers between devices: 85.1 us -> 0 us
  Pallas kernels: 0 us -> 78.4 us
  local copies, waits for them, and re-layouts: 41 us -> 2.32 us
  other arithmetic: 26.1 us -> 2.33 us
  between operations: 14.1 us -> 0.07 us
  matrix products: 24.3 us -> 13.6 us
  starting transfers between devices: 5.46 us -> 0 us
    pallas_call x0 -> x2, Pallas kernels: none -> 78.4 us  [the longest x1 50.9 us: body(): pl.pallas_call(lambda *refs: front_kernel(n_sp, n_tp, *refs), out_shape=(...]
    all_gather x5 -> x0, blocking collectives: 62.1 us -> none  [the longest x1 17.1 us: body(): lax.all_gather(narrow_end[None], 'sp', axis=0, tiled=True)]
    all_to_all x1 -> x0, waiting for transfers between devices: 58.9 us -> none  [body(): lax.all_to_all(partial_value, 'sp', split_axis=0, concat_axis=0, tiled=True)]
    all_to_all x1 -> x0, blocking collectives: 38.5 us -> none  [body(): lax.all_to_all(outgoing, 'sp', split_axis=0, concat_axis=0, tiled=True)]
    reduce_scatter x1 -> x0, waiting for transfers between devices: 26.1 us -> none  [body(): routed = lax.psum_scatter(local_sum, 'tp', scatter_dimension=1, tiled=True)]
    gather x4 -> x0, local copies, waits for them, and re-layouts: 13.2 us -> none  [the longest x2 8.77 us: body(): jnp.take(handed_back.reshape(experts * capacity, -1), positions, axis=0)]
    dot_general x22 -> x3, matrix products: 24.3 us -> 13.6 us  [the longest x1 8.15 us: body(): part = jnp.dot(hidden, w_down[0], preferred_element_type=F32).astype(BF16)]
    reduce_sum x4 -> x1, other arithmetic: 8.33 us -> 0.84 us  [body(): weight = jnp.sum(jnp.where(hits, route_weight[:, :, None], 0.0), axis=1)]
  transfers between devices with their start and end apart: 3 -> 0, of which waited for: 2 -> 0; matrix products, arithmetic and copies ran while one was open for 12% -> 0% of each run, Pallas kernels for 0% -> 0%
where the time goes in v1:
time: 96.9 us; the launch traced here: 96.7 us
  Pallas kernels  78.4 us (81%)
  matrix products  13.6 us (14%)
  other arithmetic  2.33 us (2%)
  local copies, waits for them, and re-layouts  2.32 us (2%)
    pallas_call x1, Pallas kernels, body(): pl.pallas_call(lambda *refs: front_kernel(n_sp, n_tp, *refs), out_shape=(...  50.9 us
    pallas_call x1, Pallas kernels, body(): pl.pallas_call(lambda *refs: back_kernel(n_sp, n_tp, *refs), out_shape=ja...  27.5 us
    dot_general x1, matrix products, body(): part = jnp.dot(hidden, w_down[0], preferred_element_type=F32).astype(BF16)  8.15 us
    dot_general x1, matrix products, body(): gate_proj = jnp.dot(rows, w_gate[0], preferred_element_type=F32)  4.56 us

profile of v1, /device:TPU:1, one launch (start us, length us, event | category | flops | bytes accessed | tf_op | source)
XLA Modules:
  0.0 96.7 jit_solution(2194562830800063763)
XLA Ops:
  0.0 0.8 compare_reduce_fusion
  0.8 0.8 fusion.16
  1.7 0.9 select_convert_fusion
  2.6 0.7 subtract_convert_fusion.refs_2_
  3.3 0.7 copy.21.refs_12_
  4.0 50.9 %front.1 = (bf16[128,512]{1,0:T(8,128)(2,1)}, bf16[384,2048]{1,0:T(8,128)(2,1)}) custom-call(bf16[128,512]{1,0:T(8,128)(2,1)} %refs_0_.1, bf16[128,256]{1,0:T(8,128)(2,1)} %refs_1_.1, bf16[128,512]{1,0:T(8,128)(2,1)} %refs_2_.1, bf16[128,256]{1,0:T(8,128)(2,1)} %refs_3_.1, f32[1,512]{1,0:T(1,128)} %bitcast.24, f32[1,256]{1,0:T(1,128)} %bitcast.27, ...), custom_call_target="tpu_custom_call" | custom-call | tf_op jit(solution)/shard_map/front/pallas_call | solution.py:449
  54.9 0.0 copy-start
  54.9 4.6 %fusion.4 = f32[384,1024]{1,0:T(8,128)S(1)} fusion(bf16[384,2048]{1,0:T(8,128)(2,1)} %get-tuple-element.7, bf16[1,2048,1024]{2,1,0:T(8,128)(2,1)} %param.31), kind=kOutput, calls=%fused_computation.4 | convolution fusion | flops 1610612736 | bytes 7340032 | tf_op jit(solution)/shard_map/dot_general | solution.py:502
  59.5 0.0 copy-done
  59.5 8.1 %fusion.6.refs_0_ = bf16[384,2048]{1,0:T(8,128)(2,1)} fusion(bf16[1,1024,2048]{2,1,0:T(8,128)(2,1)} %param.33, f32[384,1024]{1,0:T(8,128)S(1)} %fusion.4, bf16[384,2048]{1,0:T(8,128)(2,1)S(1)} %copy-done, bf16[1,2048,1024]{2,1,0:T(8,128)(2,1)} %param.32), kind=kOutput, calls=%fused_computation.6 | convolution fusion | flops 3224371200 | bytes 13107200 | tf_op jit(solution)/shard_map/dot_general | solution.py:505
  67.6 27.5 %back.1 = bf16[128,512]{1,0:T(8,128)(2,1)} custom-call(bf16[384,2048]{1,0:T(8,128)(2,1)} %fusion.6.refs_0_, bf16[128,384]{1,0:T(8,128)(2,1)} %get-tuple-element.9.refs_1_, bf16[128,384]{1,0:T(8,128)(2,1)} %subtract_convert_fusion.refs_2_, bf16[128,512]{1,0:T(8,128)(2,1)} %get-tuple-element.8.refs_3_), custom_call_target="tpu_custom_call" | custom-call | tf_op jit(solution)/shard_map/back/pallas_call | solution.py:506
  95.1 1.6 %copy.23 = bf16[128,512]{1,0:T(8,128)(2,1)} copy(bf16[128,512]{1,0:T(8,128)(2,1)} %back.1) | data formatting | bytes 262144
  (4 shorter events, 0.0 us)
Async XLA Ops:
  54.9 4.6 %copy-start = (bf16[384,2048]{1,0:T(8,128)(2,1)S(1)}, bf16[384,2048]{1,0:T(8,128)(2,1)}, u32[]{:S(2)}) copy-start(bf16[384,2048]{1,0:T(8,128)(2,1)} %get-tuple-element.7) | copy-start | bytes 4718596
